TPU v7x, 32 devices: a whole 2x2x4 slice. The times are simulated.
32 devices in a mesh: ep: 8 (over z, core), tp: 4 (over y, x).
Axes of the slice: x: 2, y: 2, z: 4, core: 2. Of those that a mesh axis runs over, the one named last changes fastest.
Arguments:
- tokens: bfloat16 [384, 2048], P('ep'), may hold values from -6 to 6
- retention_state: float32 [384, 16, 64, 64], P('ep', 'tp'), may hold values from -1.5 to 1.5
- lengths: int32 [384], P('ep'), may hold values from 1024 to 16383
- query_weight: bfloat16 [2048, 1024], P(None, 'tp'), may hold values from -0.125 to 0.125
- key_weight: bfloat16 [2048, 1024], P(None, 'tp'), may hold values from -0.125 to 0.125
- value_weight: bfloat16 [2048, 1024], P(None, 'tp'), may hold values from -0.125 to 0.125
- gate_weight: bfloat16 [2048, 1024], P(None, 'tp'), may hold values from -0.125 to 0.125
- out_weight: bfloat16 [1024, 2048], P(None, 'tp'), may hold values from -0.1875 to 0.1875
- first_gain: float32 [2048], replicated, may hold values from 0.1 to 1.9
- routing: int32 [384, 4], P('ep'), may hold values from 0 to 31, all different within a row; in each aligned block of 48 rows (0 to 47, 48 to 95, ...) at most 18 rows name the same one
- route_weight: float32 [384, 4], P('ep'), may hold values from 0.1 to 1
- expert_gate: bfloat16 [32, 2048, 512], P('ep', None, 'tp'), may hold values from -0.125 to 0.125
- expert_up: bfloat16 [32, 2048, 512], P('ep', None, 'tp'), may hold values from -0.125 to 0.125
- expert_down: bfloat16 [32, 512, 2048], P('ep', None, 'tp'), may hold values from -0.25 to 0.25
- shared_gate: bfloat16 [2048, 512], P(None, 'tp'), may hold values from -0.125 to 0.125
- shared_up: bfloat16 [2048, 512], P(None, 'tp'), may hold values from -0.125 to 0.125
- shared_down: bfloat16 [512, 2048], P(None, 'tp'), may hold values from -0.25 to 0.25
- side_gate: bfloat16 [2048, 256], P('ep', 'tp'), may hold values from -0.125 to 0.125
- side_up: bfloat16 [2048, 256], P('ep', 'tp'), may hold values from -0.125 to 0.125
- side_down: bfloat16 [256, 2048], P(None, 'tp'), may hold values from -0.375 to 0.375
- side_switch: bfloat16 [2048], replicated, may hold values from -0.125 to 0.125
- second_gain: float32 [2048], P('tp'), may hold values from 0.1 to 1.9
Outputs:
- output: bfloat16 [384, 2048], P('ep', 'tp')
- new_state: float32 [384, 16, 64, 64], P('ep', 'tp')
Inputs may be any that keep to these rules, and one draw needn't show every extreme that they name: `routing`: each row names 4 different experts. Among the rows of one ep index (aligned blocks of 48 rows) no expert is named by more than 18 rows, a bound that some block reaches.
All inputs are finite; a program needn't handle non-finite values.
Results may differ from a plain program's by a relative error of at most 0.013.
Values may be sent and summed in bfloat16 or wider, within the bound.
A program may use at most 64 MiB of HBM per device.

v0:
```python
import jax
import jax.numpy as jnp
from jax import lax
from jax.sharding import PartitionSpec as P

HEADS = 16


RESIDUAL_SCALE = 2.0**0.25
NORM_EPS = 1e-05
GROUP_EPS = 1e-06
ROPE_BASE = 10000.0


def rotate(vector, positions):
    half_width = vector.shape[-1] // 2
    frequency = ROPE_BASE ** (-jnp.arange(half_width, dtype=jnp.float32) / half_width)
    angles = positions.astype(jnp.float32)[:, None, None] * frequency[None, None, :]
    cosine = jnp.cos(angles)
    sine_part = jnp.sin(angles)
    first_half = vector[..., :half_width]
    second_half = vector[..., half_width:]
    return jnp.concatenate(
        [
            first_half * cosine - second_half * sine_part,
            second_half * cosine + first_half * sine_part,
        ],
        -1,
    )


def retain(
    tokens,
    retention_state,
    lengths,
    query_weight,
    key_weight,
    value_weight,
    gate_weight,
    first_head,
):
    row_count = tokens.shape[0]
    head_count = retention_state.shape[1]
    head_width = retention_state.shape[2]

    def project(weight):
        rounded = jnp.dot(tokens, weight, preferred_element_type=jnp.float32).astype(jnp.bfloat16)
        return lax.optimization_barrier(rounded).astype(jnp.float32)

    queries = rotate(project(query_weight).reshape(row_count, head_count, head_width), lengths)
    key_rows = rotate(
        project(key_weight).reshape(row_count, head_count, head_width), lengths
    ) * head_width ** (-0.5)
    values = project(value_weight).reshape(row_count, head_count, head_width)
    gate_act = project(gate_weight)
    head_index = (first_head + jnp.arange(head_count)).astype(jnp.float32)
    decays = 1.0 - 2.0 ** (-5.0 - 7.0 * head_index / (HEADS - 1))
    own_term = jnp.sum(queries * key_rows, -1, keepdims=True) * values
    carried = decays[None, :, None] * jnp.einsum(
        "bhd,bhde->bhe", queries, retention_state, precision=lax.Precision.HIGHEST
    )
    result = own_term + carried
    new_state = (
        decays[None, :, None, None] * retention_state
        + key_rows[:, :, :, None] * values[:, :, None, :]
    )
    normed = result * lax.rsqrt(jnp.mean(result * result, -1, keepdims=True) + GROUP_EPS)
    mixed_heads = (
        normed.reshape(row_count, head_count * head_width) * jax.nn.silu(gate_act)
    ).astype(jnp.bfloat16)
    return (mixed_heads, new_state)


def slot_numbers(route_ids, expert_count, capacity):
    onehot = (route_ids[..., None] == jnp.arange(expert_count, dtype=jnp.int32)).astype(jnp.int32)
    position = jnp.sum(jnp.cumsum(onehot, -2) * onehot, -1) - 1
    return route_ids * capacity + position


def on_device(
    tokens,
    retention_state,
    lengths,
    query_weight,
    key_weight,
    value_weight,
    gate_weight,
    out_weight,
    first_gain,
    routing,
    route_weight,
    expert_gate,
    expert_up,
    expert_down,
    shared_gate,
    shared_up,
    shared_down,
    side_gate,
    side_up,
    side_down,
    side_switch,
    second_gain,
):
    seq_rows = tokens.shape[0]
    model_width = tokens.shape[1]
    head_count = retention_state.shape[1]
    col_count = out_weight.shape[1]
    ep_count = lax.axis_size("ep")
    tp_rank = lax.axis_index("tp")
    col_start = tp_rank * col_count
    mixed_heads, new_state = retain(
        tokens,
        retention_state,
        lengths,
        query_weight,
        key_weight,
        value_weight,
        gate_weight,
        tp_rank * head_count,
    )
    mixing = jnp.dot(
        lax.all_gather(mixed_heads, "tp", axis=1, tiled=True),
        out_weight,
        preferred_element_type=jnp.float32,
    )
    own_cols = lax.dynamic_slice_in_dim(tokens, col_start, col_count, 1).astype(jnp.float32)
    pre_first = RESIDUAL_SCALE * own_cols + mixing
    whole_rows = lax.all_gather(pre_first, "tp", axis=1, tiled=True)
    row_mean = jnp.mean(whole_rows, -1, keepdims=True)
    square = jnp.mean(whole_rows * whole_rows, -1, keepdims=True)
    normed_full = (
        (whole_rows - row_mean) * lax.rsqrt(square - row_mean * row_mean + NORM_EPS) * first_gain
    ).astype(jnp.bfloat16)
    normed_cols = lax.dynamic_slice_in_dim(normed_full, col_start, col_count, 1)
    side_pre = jnp.dot(
        normed_full,
        lax.all_gather(side_gate, "ep", axis=0, tiled=True),
        preferred_element_type=jnp.float32,
    )
    side_lift = jnp.dot(
        normed_full,
        lax.all_gather(side_up, "ep", axis=0, tiled=True),
        preferred_element_type=jnp.float32,
    )
    side_hidden = (jax.nn.silu(side_pre) * side_lift).astype(jnp.bfloat16)
    shared_hidden = (
        jax.nn.silu(jnp.dot(normed_full, shared_gate, preferred_element_type=jnp.float32))
        * jnp.dot(normed_full, shared_up, preferred_element_type=jnp.float32)
    ).astype(jnp.bfloat16)
    shared_all, side_all = (
        lax.all_gather(shared_hidden, "tp", axis=1, tiled=True),
        lax.all_gather(side_hidden, "tp", axis=1, tiled=True),
    )
    shared_out = jnp.dot(shared_all, shared_down, preferred_element_type=jnp.float32)
    side_out = jnp.dot(side_all, side_down, preferred_element_type=jnp.float32)
    switch = jax.nn.sigmoid(jnp.dot(normed_full, side_switch, preferred_element_type=jnp.float32))
    top_count = routing.shape[1]
    local_experts = expert_gate.shape[0]
    expert_count = local_experts * ep_count
    capacity = (3 * seq_rows * top_count + expert_count - 1) // expert_count
    assigned = seq_rows * top_count
    slot_ids = slot_numbers(routing.reshape(assigned), expert_count, capacity)
    slot_hot = (
        slot_ids[:, None] == jnp.arange(expert_count * capacity, dtype=jnp.int32)[None, :]
    ).astype(jnp.bfloat16)
    token_hot = (
        (jnp.arange(assigned, dtype=jnp.int32) // top_count)[:, None]
        == jnp.arange(seq_rows, dtype=jnp.int32)[None, :]
    ).astype(jnp.bfloat16)
    every_rows, every_route = (
        lax.all_gather(normed_full, "ep", axis=0, tiled=True),
        lax.all_gather(routing, "ep", axis=0, tiled=True),
    )
    groups = every_route.reshape(ep_count, assigned)
    local_slot = (
        slot_numbers(groups, expert_count, capacity)
        - lax.axis_index("ep") * local_experts * capacity
    )
    local_hot = (
        local_slot[:, :, None]
        == jnp.arange(local_experts * capacity, dtype=jnp.int32)[None, None, :]
    ).astype(jnp.bfloat16)
    local_table = jnp.einsum(
        "gal,at->glt", local_hot, token_hot, preferred_element_type=jnp.float32
    ).astype(jnp.bfloat16)
    chosen = jnp.einsum(
        "glt,gtd->gld",
        local_table,
        every_rows.reshape(ep_count, seq_rows, model_width),
        preferred_element_type=jnp.float32,
    ).astype(jnp.bfloat16)
    slot_rows = chosen.reshape(ep_count * local_experts, capacity, model_width)
    slot_count = slot_rows.shape[1]
    grouped = slot_rows.reshape(ep_count, local_experts, slot_count, slot_rows.shape[2])
    gate_part = jnp.einsum(
        "sjcd,jdf->sjcf", grouped, expert_gate, preferred_element_type=jnp.float32
    )
    up_part = jnp.einsum("sjcd,jdf->sjcf", grouped, expert_up, preferred_element_type=jnp.float32)
    hidden = (jax.nn.silu(gate_part) * up_part).astype(jnp.bfloat16)
    hidden_all = lax.all_gather(hidden, "tp", axis=3, tiled=True)
    result = jnp.einsum(
        "sjcf,jfd->sjcd", hidden_all, expert_down, preferred_element_type=jnp.float32
    ).astype(jnp.bfloat16)
    returned = lax.all_to_all(
        result.reshape(ep_count * local_experts, slot_count, col_count),
        "ep",
        split_axis=0,
        concat_axis=0,
        tiled=True,
    )
    picked = jnp.dot(
        slot_hot,
        returned.reshape(expert_count * capacity, col_count),
        preferred_element_type=jnp.float32,
    ).reshape(seq_rows, top_count, col_count)
    routed = jnp.sum(picked * route_weight[:, :, None], 1)
    pre_second = (
        RESIDUAL_SCALE * normed_cols.astype(jnp.float32)
        + routed
        + shared_out
        + switch[:, None] * side_out
    )
    totals_second = lax.psum((jnp.sum(pre_second, -1), jnp.sum(pre_second * pre_second, -1)), "tp")
    mean_second = totals_second[0][:, None] / model_width
    square_second = totals_second[1][:, None] / model_width
    output = (
        (pre_second - mean_second)
        * lax.rsqrt(square_second - mean_second * mean_second + NORM_EPS)
        * second_gain
    ).astype(jnp.bfloat16)
    return (output, new_state)


def solution(mesh):
    return jax.shard_map(
        on_device,
        mesh=mesh,
        in_specs=(
            P("ep", None),
            P("ep", "tp", None, None),
            P("ep"),
            P(None, "tp"),
            P(None, "tp"),
            P(None, "tp"),
            P(None, "tp"),
            P(None, "tp"),
            P(),
            P("ep", None),
            P("ep", None),
            P("ep", None, "tp"),
            P("ep", None, "tp"),
            P("ep", None, "tp"),
            P(None, "tp"),
            P(None, "tp"),
            P(None, "tp"),
            P("ep", "tp"),
            P("ep", "tp"),
            P(None, "tp"),
            P(),
            P("tp"),
        ),
        out_specs=(P("ep", "tp"), P("ep", "tp", None, None)),
        check_vma=False,
    )
```

profile of v0, /device:TPU:0, one launch (start us, length us, event | category | flops | bytes accessed | tf_op | source)
XLA Modules:
  0.0 177.6 jit_solution(16361127171532134262)
XLA Ops:
  8.1 2.3 %convolution_convert_fusion.5 = bf16[48,256]{1,0:T(8,128)(2,1)} fusion(bf16[48,2048]{1,0:T(8,128)(2,1)} %param.22, bf16[2048,256]{1,0:T(8,128)(2,1)} %param.25), kind=kOutput, calls=%fused_computation.27 | convolution fusion | flops 50343936 | bytes 1269760 | tf_op jit(solution)/shard_map/dot_general | solution.py:47
  10.4 2.2 %convolution_convert_fusion.4 = bf16[48,256]{1,0:T(8,128)(2,1)} fusion(bf16[48,2048]{1,0:T(8,128)(2,1)} %param.22, bf16[2048,256]{1,0:T(8,128)(2,1)} %param.26), kind=kOutput, calls=%fused_computation.26 | convolution fusion | flops 50343936 | bytes 1269760 | tf_op jit(solution)/shard_map/dot_general | solution.py:47
  16.3 7.5 %fusion.59 = f32[48,4,1,64]{3,2,1,0:T(1,128)S(1)} fusion(f32[48,4,64,1]{2,3,1,0:T(1,128)S(1)} %bitcast.130, f32[48,4,64,64]{3,2,1,0:T(8,128)} %param.23), kind=kOutput, calls=%fused_computation.105 | convolution fusion | flops 9437184 | bytes 3244032 | tf_op jit(solution)/shard_map/bhd,bhde->bhe/dot_general | solution.py:59
  24.9 1.6 reshape.259
  27.3 10.9 %all_gather.27 = bf16[48,1024]{1,0:T(8,128)(2,1)} all-gather(bf16[48,256]{1,0:T(8,128)(2,1)S(1)} %fusion.47), channel_id=1, replica_groups=mesh['ep'=8,'tp'=4] {'tp'}, dimensions={1}, use_global_device_ids=true | all-gather | bytes 122880 | tf_op jit(solution)/shard_map/all_gather | solution.py:122
  38.2 1.2 convolution_add_fusion
  39.4 9.4 %all_gather.28 = f32[48,2048]{1,0:T(8,128)S(1)} all-gather(f32[48,512]{1,0:T(8,128)S(1)} %convolution_add_fusion), channel_id=1, replica_groups=mesh['ep'=8,'tp'=4] {'tp'}, dimensions={1}, use_global_device_ids=true | all-gather | bytes 491520 | tf_op jit(solution)/shard_map/all_gather | solution.py:128
  49.9 13.2 %all-gather = s32[8,48,4]{1,2,0:T(4,128)S(1)} all-gather(s32[1,48,4]{1,2,0:T(4,128)S(1)} %bitcast.133), channel_id=1, replica_groups=mesh['ep'=8,'tp'=4] {'ep'}, dimensions={0}, use_global_device_ids=true | all-gather | bytes 6912 | tf_op jit(solution)/shard_map/all_gather | solution.py:172
  65.9 4.6 %reduce-window.16 = s32[8,32,2,128]{3,1,2,0:T(8,128)S(1)} reduce-window(s32[8,32,2,128]{3,1,2,0:T(8,128)S(1)} %copy_bitcast_fusion, s32[]{:T(128)} %constant.71.clone.1), window={size=1x1x1x128 pad=0_0x0_0x0_0x127_0}, to_apply=%region_7.8 | reduce-window | flops 8323072 | bytes 524292 | tf_op jit(solution)/shard_map/reduce-window.2
  73.0 14.4 %all_gather.33 = bf16[2048,64]{0,1:T(8,128)(2,1)S(1)} all-gather(bf16[256,64]{0,1:T(8,128)(2,1)} %param.39), channel_id=1, replica_groups=mesh['ep'=8,'tp'=4] {'ep'}, dimensions={0}, use_global_device_ids=true | all-gather | bytes 294912 | tf_op jit(solution)/shard_map/all_gather | solution.py:137
  87.4 14.6 %all_gather.34 = bf16[2048,64]{0,1:T(8,128)(2,1)S(1)} all-gather(bf16[256,64]{0,1:T(8,128)(2,1)} %param.40), channel_id=1, replica_groups=mesh['ep'=8,'tp'=4] {'ep'}, dimensions={0}, use_global_device_ids=true | all-gather | bytes 294912 | tf_op jit(solution)/shard_map/all_gather | solution.py:142
  104.0 3.8 %convolution_convert_fusion = bf16[8,72,2048]{2,1,0:T(8,128)(2,1)} fusion(bf16[8,48,2048]{2,1,0:T(8,128)(2,1)} %bitcast.129, s32[8,192]{1,0:T(8,128)S(1)} %add_subtract_fusion, s32[192]{0:T(256)} %and_select_fusion), kind=kOutput, calls=%fused_computation.2 | convolution fusion | flops 125190144 | bytes 3939072 | tf_op jit(solution)/shard_map/glt,gtd->gld/dot_general | solution.py:186
  107.9 3.1 %copy.95 = bf16[8,72,2048]{2,0,1:T(8,128)(2,1)S(1)} copy(bf16[8,72,2048]{2,1,0:T(8,128)(2,1)} %convolution_convert_fusion) | data formatting | bytes 4718592 | tf_op jit(solution)/shard_map/convert_element_type | solution.py:191
  113.4 10.4 %all_gather.31 = bf16[8,4,18,512]{3,0,2,1:T(8,128)(2,1)S(1)} all-gather(bf16[8,4,18,128]{3,0,2,1:T(8,128)(2,1)S(1)} %fusion.23), channel_id=1, replica_groups=mesh['ep'=8,'tp'=4] {'tp'}, dimensions={3}, use_global_device_ids=true | all-gather | bytes 737280 | tf_op jit(solution)/shard_map/all_gather | solution.py:200
  125.5 3.5 %all-to-all-start = ((bf16[32,18,512]{2,1,0:T(8,128)(2,1)}), bf16[32,18,512]{2,1,0:T(8,128)(2,1)S(1)}, u32[]{:S(2)}, u32[]{:S(2)}) async-start(bf16[32,18,512]{2,1,0:T(8,128)(2,1)} %bitcast.22), calls=%async_computation | async-start | bytes 1572864 | tf_op jit(solution)/shard_map/all_to_all | solution.py:204
  129.0 1.6 fusion.31
  132.1 7.6 %all-gather.1 = bf16[4,64,48]{1,2,0:T(8,128)(2,1)S(1)} all-gather(bf16[1,64,48]{1,2,0:T(8,128)(2,1)} %fusion.31), channel_id=1, replica_groups=mesh['ep'=8,'tp'=4] {'tp'}, dimensions={0}, use_global_device_ids=true | all-gather | bytes 30720 | tf_op jit(solution)/shard_map/all_gather | solution.py:152
  140.5 8.4 %all_gather.32 = bf16[48,512]{1,0:T(8,128)(2,1)} all-gather(bf16[48,128]{1,0:T(8,128)(2,1)S(1)} %fusion.29), channel_id=1, replica_groups=mesh['ep'=8,'tp'=4] {'tp'}, dimensions={1}, use_global_device_ids=true | all-gather | bytes 61440 | tf_op jit(solution)/shard_map/all_gather | solution.py:151
  149.0 7.4 %multiply_add_fusion = f32[48,4,64,64]{3,2,1,0:T(8,128)} fusion(f32[48,4,64,64]{3,2,1,0:T(8,128)} %param.23, f32[48,4,64]{2,1,0:T(4,128)S(1)} %reshape.273, f32[48,4,64]{2,1,0:T(4,128)S(1)} %get-tuple-element.24, f32[4]{0:T(128)} %copy-done.17), kind=kLoop, calls=%fused_computation.1 | loop fusion | flops 2359296 | bytes 6389776 | tf_op jit(solution)/shard_map/add | solution.py:64
  156.4 1.0 reshape.287
  157.4 1.4 fusion.22
  158.9 1.2 convolution_add_fusion.1
  160.1 1.0 fusion.58
  161.1 8.9 %all-reduce.2 = (f32[48]{0:T(128)S(1)}, f32[48]{0:T(128)S(1)}) all-reduce(f32[48]{0:T(128)S(1)} %get-tuple-element.5, f32[48]{0:T(128)S(1)} %get-tuple-element.4), channel_id=1, replica_groups=mesh['ep'=8,'tp'=4] {'tp'}, use_global_device_ids=true, to_apply=%region_14.15 | all-reduce | flops 96 | bytes 768 | tf_op jit(solution)/shard_map/psum | solution.py:223
  (102 shorter events, 21.7 us)
Async XLA Ops:
  7.2 116.6 %copy-start = (bf16[4,512,512]{2,1,0:T(8,128)(2,1)S(1)}, bf16[4,512,512]{2,1,0:T(8,128)(2,1)}, u32[]{:S(2)}) copy-start(bf16[4,512,512]{2,1,0:T(8,128)(2,1)} %param.35) | copy-start | bytes 6291460
  7.2 5.5 %copy-start.3 = (bf16[48,2048]{1,0:T(8,128)(2,1)S(1)}, bf16[48,2048]{1,0:T(8,128)(2,1)}, u32[]{:S(2)}) copy-start(bf16[48,2048]{1,0:T(8,128)(2,1)} %param.22) | copy-start | bytes 589828
  7.2 5.5 %copy-start.4 = (bf16[2048,256]{1,0:T(8,128)(2,1)S(1)}, bf16[2048,256]{1,0:T(8,128)(2,1)}, u32[]{:S(2)}) copy-start(bf16[2048,256]{1,0:T(8,128)(2,1)} %param.27) | copy-start | bytes 3145732
  7.2 96.8 %all-gather.4.cloned.1.call-start = ((), (), s32[]{:S(2)}) async-start(), calls=%async_computation.1 | async-start | bytes 1769472 | tf_op jit(solution)/shard_map/all_gather | solution.py:171
  7.3 5.7 %copy-start.5 = (bf16[2048,256]{1,0:T(8,128)(2,1)S(1)}, bf16[2048,256]{1,0:T(8,128)(2,1)}, u32[]{:S(2)}) copy-start(bf16[2048,256]{1,0:T(8,128)(2,1)} %param.28) | copy-start | bytes 3145732
  7.3 16.5 %copy-start.17 = (f32[4]{0:T(128)}, f32[4]{0:T(128)S(1)}, u32[]{:S(2)}) copy-start(f32[4]{0:T(128)S(1)} %power_subtract_fusion) | copy-start | bytes 52
  16.3 21.9 %copy-start.6 = (bf16[1024,512]{1,0:T(8,128)(2,1)S(1)}, bf16[1024,512]{1,0:T(8,128)(2,1)}, u32[]{:S(2)}) copy-start(bf16[1024,512]{1,0:T(8,128)(2,1)} %param.29) | copy-start | bytes 3145732
  23.8 25.2 %copy-start.15 = (f32[2048]{0:T(1024)S(1)}, f32[2048]{0:T(1024)}, u32[]{:S(2)}) copy-start(f32[2048]{0:T(1024)} %param.30) | copy-start | bytes 24580
  23.8 26.0 %copy-start.12 = (s32[48,4]{0,1:T(4,128)S(1)}, s32[48,4]{0,1:T(4,128)}, u32[]{:S(2)}) copy-start(s32[48,4]{0,1:T(4,128)} %param.31) | copy-start | bytes 2308
  49.8 53.0 %copy-start.1 = (bf16[48,2048]{1,0:T(8,128)(2,1)S(1)}, bf16[48,2048]{1,0:T(8,128)(2,1)}, u32[]{:S(2)}) copy-start(bf16[48,2048]{1,0:T(8,128)(2,1)} %multiply_convert_fusion) | copy-start | bytes 589828
  49.8 53.8 %copy-start.7 = (bf16[2048,128]{1,0:T(8,128)(2,1)S(1)}, bf16[2048,128]{1,0:T(8,128)(2,1)}, u32[]{:S(2)}) copy-start(bf16[2048,128]{1,0:T(8,128)(2,1)} %param.36) | copy-start | bytes 1572868
  63.3 0.6 copy-start.14
  64.4 0.6 copy-start.9
  70.9 32.9 %copy-start.8 = (bf16[2048,128]{1,0:T(8,128)(2,1)S(1)}, bf16[2048,128]{1,0:T(8,128)(2,1)}, u32[]{:S(2)}) copy-start(bf16[2048,128]{1,0:T(8,128)(2,1)} %param.37) | copy-start | bytes 1572868
  107.9 3.1 %copy-start.2 = (bf16[4,2048,128]{2,1,0:T(8,128)(2,1)S(1)}, bf16[4,2048,128]{2,1,0:T(8,128)(2,1)}, u32[]{:S(2)}) copy-start(bf16[4,2048,128]{2,1,0:T(8,128)(2,1)} %param.33) | copy-start | bytes 6291460
  111.0 1.6 copy-start.18
  124.5 24.3 %copy-start.13 = (s32[48,4]{0,1:T(4,128)S(1)}, s32[48,4]{0,1:T(4,128)}, u32[]{:S(2)}) copy-start(s32[48,4]{0,1:T(4,128)} %param.31) | copy-start | bytes 2308
  125.5 30.9 %all-to-all-start = ((bf16[32,18,512]{2,1,0:T(8,128)(2,1)}), bf16[32,18,512]{2,1,0:T(8,128)(2,1)S(1)}, u32[]{:S(2)}, u32[]{:S(2)}) async-start(bf16[32,18,512]{2,1,0:T(8,128)(2,1)} %bitcast.22), calls=%async_computation | async-start | bytes 1572864 | tf_op jit(solution)/shard_map/all_to_all | solution.py:204
  149.0 8.4 %copy-start.19 = (f32[48,4]{0,1:T(4,128)S(1)}, f32[48,4]{0,1:T(4,128)}, u32[]{:S(2)}) copy-start(f32[48,4]{0,1:T(4,128)} %param.32) | copy-start | bytes 2308
  156.4 2.5 %copy-start.11 = (bf16[48,512]{1,0:T(8,128)(2,1)S(1)}, bf16[48,512]{1,0:T(8,128)(2,1)}, u32[]{:S(2)}) copy-start(bf16[48,512]{1,0:T(8,128)(2,1)} %all_gather.32) | copy-start | bytes 147460
  156.4 3.7 %copy-start.10 = (bf16[256,512]{1,0:T(8,128)(2,1)S(1)}, bf16[256,512]{1,0:T(8,128)(2,1)}, u32[]{:S(2)}) copy-start(bf16[256,512]{1,0:T(8,128)(2,1)} %param.41) | copy-start | bytes 786436
  156.4 13.7 %copy-start.16 = (f32[512]{0:T(512)S(1)}, f32[512]{0:T(512)}, u32[]{:S(2)}) copy-start(f32[512]{0:T(512)} %param.43) | copy-start | bytes 6148
Sparse Core Ops, SparseCore 0:
  49.9 25.5 all-gather.3
where the time goes:
time: 179 us; the launch traced here: 178 us
  blocking collectives  97.9 us (55%)
  matrix products  27.1 us (15%)
  other arithmetic  20.6 us (12%)
  between operations  14.5 us (8%)
  local copies, waits for them, and re-layouts  14 us (8%)
  starting transfers between devices  3.58 us (2%)
    all_gather x1, blocking collectives, on_device(): lax.all_gather(side_up, 'ep', axis=0, tiled=True)  14.6 us
    all_gather x1, blocking collectives, on_device(): lax.all_gather(side_gate, 'ep', axis=0, tiled=True)  14.4 us
    all_gather x1, blocking collectives, on_device(): lax.all_gather(routing, 'ep', axis=0, tiled=True)  13.2 us
    all_gather x1, blocking collectives, on_device(): lax.all_gather(mixed_heads, 'tp', axis=1, tiled=True)  10.9 us
    all_gather x1, blocking collectives, on_device(): hidden_all = lax.all_gather(hidden, 'tp', axis=3, tiled=True)  10.4 us
    all_gather x1, blocking collectives, on_device(): whole_rows = lax.all_gather(pre_first, 'tp', axis=1, tiled=True)  9.44 us
    psum x1, blocking collectives, on_device(): lax.psum((jnp.sum(pre_second, -1), jnp.sum(pre_second * pre_second, -1)),...  8.93 us
    all_gather x1, blocking collectives, on_device(): lax.all_gather(shared_hidden, 'tp', axis=1, tiled=True)  8.35 us
  transfers between devices with their start and end apart: 2, of which 0 were waited for; matrix products, arithmetic and copies ran while one was open for 13% of the time, Pallas kernels for 0%

commit v1 on v0

v1 whole, which is shorter than its diff:
```python
import functools

import jax
import jax.numpy as jnp
from jax import lax
from jax.experimental import pallas as pl
from jax.experimental.pallas import tpu as pltpu
from jax.sharding import PartitionSpec as P

HEADS = 16


RESIDUAL_SCALE = 2.0**0.25
NORM_EPS = 1e-05
GROUP_EPS = 1e-06
ROPE_BASE = 10000.0


def rotate(vector, positions):
    half_width = vector.shape[-1] // 2
    frequency = ROPE_BASE ** (-jnp.arange(half_width, dtype=jnp.float32) / half_width)
    angles = positions.astype(jnp.float32)[:, None, None] * frequency[None, None, :]
    cosine = jnp.cos(angles)
    sine_part = jnp.sin(angles)
    first_half = vector[..., :half_width]
    second_half = vector[..., half_width:]
    return jnp.concatenate(
        [
            first_half * cosine - second_half * sine_part,
            second_half * cosine + first_half * sine_part,
        ],
        -1,
    )


def retain(
    retention_state,
    lengths,
    projections,
    first_head,
):
    row_count = retention_state.shape[0]
    head_count = retention_state.shape[1]
    head_width = retention_state.shape[2]

    query_rows, key_part, value_part, gate_part = [part.astype(jnp.float32) for part in projections]
    queries = rotate(query_rows.reshape(row_count, head_count, head_width), lengths)
    key_rows = rotate(
        key_part.reshape(row_count, head_count, head_width), lengths
    ) * head_width ** (-0.5)
    values = value_part.reshape(row_count, head_count, head_width)
    gate_act = gate_part
    head_index = (first_head + jnp.arange(head_count)).astype(jnp.float32)
    decays = 1.0 - 2.0 ** (-5.0 - 7.0 * head_index / (HEADS - 1))
    own_term = jnp.sum(queries * key_rows, -1, keepdims=True) * values
    carried = decays[None, :, None] * jnp.sum(queries[:, :, :, None] * retention_state, 2)
    result = own_term + carried
    new_state = (
        decays[None, :, None, None] * retention_state
        + key_rows[:, :, :, None] * values[:, :, None, :]
    )
    normed = result * lax.rsqrt(jnp.mean(result * result, -1, keepdims=True) + GROUP_EPS)
    mixed_heads = (
        normed.reshape(row_count, head_count * head_width) * jax.nn.silu(gate_act)
    ).astype(jnp.bfloat16)
    return (mixed_heads, new_state)


VMEM = pl.BlockSpec(memory_space=pltpu.VMEM)
DEVICE = pl.DeviceIdType.MESH


def enter(peers):
    barrier = pltpu.get_barrier_semaphore()
    for peer in peers:
        pl.semaphore_signal(barrier, inc=1, device_id=peer, device_id_type=DEVICE)
    pl.semaphore_wait(barrier, len(peers))


def send(source, target, send_sem, recv_sem, peer):
    copy = pltpu.make_async_remote_copy(
        src_ref=source,
        dst_ref=target,
        send_sem=send_sem,
        recv_sem=recv_sem,
        device_id=peer,
        device_id_type=DEVICE,
    )
    copy.start()
    return copy


def on_axis(axis, index):
    if axis == "ep":
        return (index, lax.axis_index("tp"))
    return (lax.axis_index("ep"), index)


def gather_body(axis, count, parts, *refs):
    sources, targets = refs[:parts], refs[parts : 2 * parts]
    send_sem, recv_sem, local_sem = refs[2 * parts :]
    me = lax.axis_index(axis)
    others = [lax.rem(me + step, count) for step in range(1, count)]
    locals_ = []
    for part in range(parts):
        own = pltpu.make_async_copy(sources[part], targets[part].at[me], local_sem.at[part])
        own.start()
        locals_.append(own)
    enter([on_axis(axis, other) for other in others])
    copies = []
    for step, other in enumerate(others):
        for part in range(parts):
            copies.append(
                send(
                    sources[part],
                    targets[part].at[me],
                    send_sem.at[step, part],
                    recv_sem.at[step, part],
                    on_axis(axis, other),
                )
            )
    for copy in locals_:
        copy.wait()
    for copy in copies:
        copy.wait()


def gather(arrays, axis, ident):
    count, parts = lax.axis_size(axis), len(arrays)
    return pl.pallas_call(
        functools.partial(gather_body, axis, count, parts),
        out_shape=[jax.ShapeDtypeStruct((count,) + a.shape, a.dtype) for a in arrays],
        in_specs=[VMEM] * parts,
        out_specs=[VMEM] * parts,
        scratch_shapes=[
            pltpu.SemaphoreType.DMA((count - 1, parts)),
            pltpu.SemaphoreType.DMA((count - 1, parts)),
            pltpu.SemaphoreType.DMA((parts,)),
        ],
        compiler_params=pltpu.CompilerParams(collective_id=ident, has_side_effects=True),
    )(*arrays)


def scatter_body(count, source, target, send_sem, recv_sem, local_sem):
    me = lax.axis_index("ep")
    others = [lax.rem(me + step, count) for step in range(1, count)]
    own = pltpu.make_async_copy(source.at[me], target.at[me], local_sem)
    own.start()
    enter([on_axis("ep", other) for other in others])
    copies = [
        send(
            source.at[other],
            target.at[me],
            send_sem.at[step],
            recv_sem.at[step],
            on_axis("ep", other),
        )
        for step, other in enumerate(others)
    ]
    own.wait()
    for copy in copies:
        copy.wait()


def scatter(array, ident):
    count = array.shape[0]
    return pl.pallas_call(
        functools.partial(scatter_body, count),
        out_shape=jax.ShapeDtypeStruct(array.shape, array.dtype),
        in_specs=[VMEM],
        out_specs=VMEM,
        scratch_shapes=[
            pltpu.SemaphoreType.DMA((count - 1,)),
            pltpu.SemaphoreType.DMA((count - 1,)),
            pltpu.SemaphoreType.DMA,
        ],
        compiler_params=pltpu.CompilerParams(collective_id=ident, has_side_effects=True),
    )(array)


def first_body(count, *refs):
    parts = 3
    sources, (tokens, *weights) = refs[:parts], refs[parts : parts + 5]
    targets = refs[parts + 5 : 2 * parts + 5]
    results = refs[2 * parts + 5 : 2 * parts + 9]
    send_sem, recv_sem, local_sem = refs[2 * parts + 9 :]
    chips = count // 2
    me = lax.axis_index("ep")
    chip, core = me // 2, lax.rem(me, 2)
    partner = on_axis("ep", chip * 2 + 1 - core)
    line = [lax.rem(chip + step, chips) * 2 + core for step in range(1, chips)]
    senders = [lax.rem(chip + chips - step, chips) * 2 + core for step in range(1, chips)]
    locals_ = []
    for part in range(parts):
        own = pltpu.make_async_copy(sources[part], targets[part].at[me], local_sem.at[part])
        own.start()
        locals_.append(own)
    enter([on_axis("ep", other) for other in line] + [partner])
    direct, copies = [], []
    for step, other in enumerate(line):
        for part in range(parts):
            direct.append(
                send(
                    sources[part],
                    targets[part].at[me],
                    send_sem.at[step, part],
                    recv_sem.at[step, part],
                    on_axis("ep", other),
                )
            )
    for part in range(parts):
        copies.append(
            send(
                sources[part],
                targets[part].at[me],
                send_sem.at[chips - 1, part],
                recv_sem.at[chips - 1, part],
                partner,
            )
        )
    for weight, result in zip(weights, results):
        result[...] = jnp.dot(
            tokens[...], weight[...], preferred_element_type=jnp.float32
        ).astype(result.dtype)
    for step, sender in enumerate(senders):
        for part in range(parts):
            direct[step * parts + part].wait_recv()
            copies.append(
                send(
                    targets[part].at[sender],
                    targets[part].at[sender],
                    send_sem.at[chips + step, part],
                    recv_sem.at[chips + step, part],
                    partner,
                )
            )
    for copy in locals_:
        copy.wait()
    for copy in direct:
        copy.wait_send()
    for copy in copies:
        copy.wait()


def first(arrays, tokens, weights, ident):
    count, parts = lax.axis_size("ep"), len(arrays)
    rows = tokens.shape[0]
    return pl.pallas_call(
        functools.partial(first_body, count),
        out_shape=[jax.ShapeDtypeStruct((count,) + a.shape, a.dtype) for a in arrays]
        + [jax.ShapeDtypeStruct((rows, w.shape[1]), jnp.bfloat16) for w in weights],
        in_specs=[VMEM] * (parts + 5),
        out_specs=[VMEM] * (parts + 4),
        scratch_shapes=[
            pltpu.SemaphoreType.DMA((count - 1, parts)),
            pltpu.SemaphoreType.DMA((count - 1, parts)),
            pltpu.SemaphoreType.DMA((parts,)),
        ],
        compiler_params=pltpu.CompilerParams(collective_id=ident, has_side_effects=True),
    )(*arrays, tokens, *weights)


def spread_body(count, tp_count, source, target, send_sem, recv_sem, local_sem):
    chips, width = count // 2, source.shape[1]
    me, own_tp = lax.axis_index("ep"), lax.axis_index("tp")
    chip, core = me // 2, lax.rem(me, 2)
    partner = (chip * 2 + 1 - core, own_tp)

    def place(row, col):
        return target.at[row, :, pl.ds(pl.multiple_of(col * width, width), width)]

    def chip_at(step):
        return lax.rem(chip + chips + step, chips) * 2 + core

    def tp_at(step):
        return lax.rem(own_tp + tp_count + step, tp_count)

    own = pltpu.make_async_copy(source, place(me, own_tp), local_sem)
    own.start()
    line = [(chip_at(step), own_tp) for step in range(1, chips)]
    plane = [(me, tp_at(step)) for step in range(1, tp_count)]
    enter(line + plane + [partner])

    def pair(line_step, plane_step, to_partner):
        return (
            send_sem.at[to_partner, line_step, plane_step],
            recv_sem.at[to_partner, line_step, plane_step],
        )

    direct, planar, copies = [], {}, []
    for step in range(1, chips):
        direct.append(send(source, place(me, own_tp), *pair(step, 0, 0), line[step - 1]))
    for step in range(1, tp_count):
        planar[(0, step)] = send(source, place(me, own_tp), *pair(0, step, 0), plane[step - 1])
    copies.append(send(source, place(me, own_tp), *pair(0, 0, 1), partner))
    for line_step in range(1, chips):
        direct[line_step - 1].wait_recv()
        block = place(chip_at(-line_step), own_tp)
        for step in range(1, tp_count):
            planar[(line_step, step)] = send(
                block, block, *pair(line_step, step, 0), plane[step - 1]
            )
        copies.append(send(block, block, *pair(line_step, 0, 1), partner))
    for line_step in range(chips):
        for step in range(1, tp_count):
            planar[(line_step, step)].wait_recv()
            block = place(chip_at(-line_step), tp_at(-step))
            copies.append(send(block, block, *pair(line_step, step, 1), partner))
    own.wait()
    for copy in direct:
        copy.wait_send()
    for copy in planar.values():
        copy.wait_send()
    for copy in copies:
        copy.wait()


def spread(block, ident):
    count, tp_count = lax.axis_size("ep"), lax.axis_size("tp")
    rows, width = block.shape
    return pl.pallas_call(
        functools.partial(spread_body, count, tp_count),
        out_shape=jax.ShapeDtypeStruct((count, rows, width * tp_count), block.dtype),
        in_specs=[VMEM],
        out_specs=VMEM,
        scratch_shapes=[
            pltpu.SemaphoreType.DMA((2, count // 2, tp_count)),
            pltpu.SemaphoreType.DMA((2, count // 2, tp_count)),
            pltpu.SemaphoreType.DMA,
        ],
        compiler_params=pltpu.CompilerParams(collective_id=ident, has_side_effects=True),
    )(block)


def side_by_side(gathered):
    return jnp.concatenate([gathered[i] for i in range(gathered.shape[0])], -1)


def row_moments(values, ident):
    sums = jnp.stack([jnp.sum(values, -1), jnp.sum(values * values, -1)])
    (every,) = gather([sums], "tp", ident)
    totals = jnp.sum(every, 0)
    return totals[0][:, None], totals[1][:, None]


def on_device(
    tokens,
    retention_state,
    lengths,
    query_weight,
    key_weight,
    value_weight,
    gate_weight,
    out_weight,
    first_gain,
    routing,
    route_weight,
    expert_gate,
    expert_up,
    expert_down,
    shared_gate,
    shared_up,
    shared_down,
    side_gate,
    side_up,
    side_down,
    side_switch,
    second_gain,
):
    seq_rows = tokens.shape[0]
    model_width = tokens.shape[1]
    head_count = retention_state.shape[1]
    col_count = out_weight.shape[1]
    ep_count = lax.axis_size("ep")
    tp_rank = lax.axis_index("tp")
    ep_rank = lax.axis_index("ep")
    col_start = tp_rank * col_count
    side_width = side_gate.shape[1]
    side_part = jnp.concatenate([side_gate, side_up], 1)
    side_both, every_route, every_weight, *projections = first(
        [side_part, routing.T, route_weight.T],
        tokens,
        [query_weight, key_weight, value_weight, gate_weight],
        0,
    )
    side_both = side_both.reshape(model_width, 2 * side_width)
    mixed_heads, new_state = retain(
        retention_state, lengths, projections, tp_rank * head_count
    )
    (every_mixed,) = gather([mixed_heads], "tp", 1)
    mixing = jnp.dot(
        side_by_side(every_mixed),
        out_weight,
        preferred_element_type=jnp.float32,
    )
    own_cols = lax.dynamic_slice_in_dim(tokens, col_start, col_count, 1).astype(jnp.float32)
    pre_first = RESIDUAL_SCALE * own_cols + mixing
    first_sum, first_square = row_moments(pre_first, 2)
    row_mean = first_sum / model_width
    square = first_square / model_width
    own_gain = lax.dynamic_slice_in_dim(first_gain, col_start, col_count, 0)
    normed_cols = (
        (pre_first - row_mean) * lax.rsqrt(square - row_mean * row_mean + NORM_EPS) * own_gain
    ).astype(jnp.bfloat16)
    every_rows = spread(normed_cols, 3)
    normed_full = lax.dynamic_index_in_dim(every_rows, ep_rank, 0, keepdims=False)
    every_rows = every_rows.reshape(ep_count * seq_rows, model_width)

    local_experts = expert_gate.shape[0]
    top_count = routing.shape[1]
    expert_count = local_experts * ep_count
    capacity = (3 * seq_rows * top_count + expert_count - 1) // expert_count
    total_rows = ep_count * seq_rows
    route_all = jnp.transpose(every_route, (1, 0, 2)).reshape(top_count, total_rows)
    weight_all = jnp.transpose(every_weight, (1, 0, 2)).reshape(top_count, total_rows)
    local_ids = ep_rank * local_experts + jnp.arange(local_experts, dtype=jnp.int32)
    named = route_all[None, :, :] == local_ids[:, None, None]
    member = jnp.any(named, 1)
    pair_weight = jnp.sum(jnp.where(named, weight_all[None, :, :], 0.0), 1)
    index = jnp.arange(total_rows, dtype=jnp.int32)
    group = index // seq_rows
    earlier = ((index[:, None] < index[None, :]) & (group[:, None] == group[None, :])).astype(
        jnp.bfloat16
    )
    before = jnp.dot(
        member.astype(jnp.bfloat16), earlier, preferred_element_type=jnp.float32
    ).astype(jnp.int32)
    slot = jnp.where(member, group[None, :] * capacity + before, -1)
    slot_total = ep_count * capacity
    hit = slot[:, None, :] == jnp.arange(slot_total, dtype=jnp.int32)[None, :, None]
    table = hit.astype(jnp.bfloat16).reshape(local_experts * slot_total, total_rows)
    slot_weight = jnp.sum(jnp.where(hit, pair_weight[:, None, :], 0.0), -1, keepdims=True)
    chosen = (
        jnp.dot(table, every_rows, preferred_element_type=jnp.float32)
        .astype(jnp.bfloat16)
        .reshape(local_experts, slot_total, model_width)
    )
    gate_part = jnp.einsum("jcd,jdf->jcf", chosen, expert_gate, preferred_element_type=jnp.float32)
    up_part = jnp.einsum("jcd,jdf->jcf", chosen, expert_up, preferred_element_type=jnp.float32)
    hidden = (jax.nn.silu(gate_part) * up_part * slot_weight).astype(jnp.bfloat16)

    side_pre = jnp.dot(normed_full, side_both, preferred_element_type=jnp.float32)
    side_hidden = (jax.nn.silu(side_pre[:, :side_width]) * side_pre[:, side_width:]).astype(
        jnp.bfloat16
    )
    shared_hidden = (
        jax.nn.silu(jnp.dot(normed_full, shared_gate, preferred_element_type=jnp.float32))
        * jnp.dot(normed_full, shared_up, preferred_element_type=jnp.float32)
    ).astype(jnp.bfloat16)
    hidden_blocks, shared_blocks, side_blocks = gather(
        [hidden.reshape(local_experts * slot_total, -1), shared_hidden, side_hidden], "tp", 4
    )
    hidden_all = side_by_side(hidden_blocks).reshape(local_experts, slot_total, -1)
    result = (
        jnp.einsum("jcf,jfd->jcd", hidden_all, expert_down, preferred_element_type=jnp.float32)
        .astype(jnp.bfloat16)
        .reshape(local_experts * slot_total, col_count)
    )
    summed = (
        lax.dot_general(
            table, result, (((0,), (0,)), ((), ())), preferred_element_type=jnp.float32
        )
        .astype(jnp.bfloat16)
        .reshape(ep_count, seq_rows, col_count)
    )
    returned = scatter(summed, 5)
    routed = jnp.sum(returned.astype(jnp.float32), 0)
    shared_out = jnp.dot(
        side_by_side(shared_blocks), shared_down, preferred_element_type=jnp.float32
    )
    side_out = jnp.dot(side_by_side(side_blocks), side_down, preferred_element_type=jnp.float32)
    switch = jax.nn.sigmoid(
        jnp.sum(normed_full.astype(jnp.float32) * side_switch.astype(jnp.float32)[None, :], -1)
    )
    pre_second = (
        RESIDUAL_SCALE * normed_cols.astype(jnp.float32)
        + routed
        + shared_out
        + switch[:, None] * side_out
    )
    second_sum, second_square = row_moments(pre_second, 6)
    mean_second = second_sum / model_width
    square_second = second_square / model_width
    output = (
        (pre_second - mean_second)
        * lax.rsqrt(square_second - mean_second * mean_second + NORM_EPS)
        * second_gain
    ).astype(jnp.bfloat16)
    return (output, new_state)


def solution(mesh):
    return jax.shard_map(
        on_device,
        mesh=mesh,
        in_specs=(
            P("ep", None),
            P("ep", "tp", None, None),
            P("ep"),
            P(None, "tp"),
            P(None, "tp"),
            P(None, "tp"),
            P(None, "tp"),
            P(None, "tp"),
            P(),
            P("ep", None),
            P("ep", None),
            P("ep", None, "tp"),
            P("ep", None, "tp"),
            P("ep", None, "tp"),
            P(None, "tp"),
            P(None, "tp"),
            P(None, "tp"),
            P("ep", "tp"),
            P("ep", "tp"),
            P(None, "tp"),
            P(),
            P("tp"),
        ),
        out_specs=(P("ep", "tp"), P("ep", "tp", None, None)),
        check_vma=False,
    )
```

time: 179 us -> 125 us (0.70)
  blocking collectives: 97.9 us -> 0 us
  Pallas kernels: 0 us -> 76.2 us
  matrix products: 27.1 us -> 11.8 us
  between operations: 14.5 us -> 1.06 us
  starting transfers between devices: 3.58 us -> 0 us
  local copies, waits for them, and re-layouts: 14 us -> 12.2 us
  other arithmetic: 20.6 us -> 22.4 us
    all_gather x8 -> x0, blocking collectives: 88.9 us -> none  [the longest x1 14.6 us: on_device(): lax.all_gather(side_up, 'ep', axis=0, tiled=True)]
    pallas_call x0 -> x7, Pallas kernels: none -> 76.2 us  [the longest x4 31.1 us: gather(): pl.pallas_call(functools.partial(gather_body, axis, count, parts), out_sh...]
    dot_general x16 -> x9, matrix products: 26.7 us -> 8.66 us  [the longest x1 1.56 us: on_device(): lax.dot_general(table, result, (((0,), (0,)), ((), ())), preferred_elemen...]
    psum x1 -> x0, blocking collectives: 8.93 us -> none  [on_device(): lax.psum((jnp.sum(pre_second, -1), jnp.sum(pre_second * pre_second, -1)),...]
    another operation x8 -> x2, other arithmetic: 6.29 us -> 1.14 us  [row_moments(): sums = jnp.stack([jnp.sum(values, -1), jnp.sum(values * values, -1)])]
    reduce_sum x3 -> x8, other arithmetic: 0.89 us -> 4.89 us  [the longest x2 1.4 us: row_moments(): totals = jnp.sum(every, 0)]
    all_to_all x1 -> x0, starting transfers between devices: 3.55 us -> none  [on_device(): lax.all_to_all(result.reshape(ep_count * local_experts, slot_count, col_c...]
    convert_element_type x1 -> x0, local copies, waits for them, and re-layouts: 3.11 us -> none  [on_device(): chosen = jnp.einsum('glt,gtd->gld', local_table, every_rows.reshape(ep_co...]
  transfers between devices with their start and end apart: 2 -> 0, of which waited for: 0 -> 0; matrix products, arithmetic and copies ran while one was open for 13% -> 0% of each run, Pallas kernels for 0% -> 0%
where the time goes in v1:
time: 125 us; the launch traced here: 124 us
  Pallas kernels  76.2 us (61%)
  other arithmetic  22.4 us (18%)
  local copies, waits for them, and re-layouts  12.2 us (10%)
  matrix products  11.8 us (9%)
    pallas_call x4, Pallas kernels, gather(): pl.pallas_call(functools.partial(gather_body, axis, count, parts), out_sh...  31.1 us
    pallas_call x1, Pallas kernels, spread(): pl.pallas_call(functools.partial(spread_body, count, tp_count), out_shape...  17.7 us
    pallas_call x1, Pallas kernels, first(): pl.pallas_call(functools.partial(first_body, count), out_shape=[jax.Shape...  15.6 us
    pallas_call x1, Pallas kernels, scatter(): pl.pallas_call(functools.partial(scatter_body, count), out_shape=jax.Shap...  11.8 us
    add x1, other arithmetic, retain(): decays[None, :, None, None] * retention_state  9.16 us
    unnamed x40, local copies, waits for them, and re-layouts  2.83 us

profile of v1, /device:TPU:0, one launch (start us, length us, event | category | flops | bytes accessed | tf_op | source)
XLA Modules:
  0.0 123.5 jit_solution(15533541414120755268)
XLA Ops:
  1.5 1.3 %dynamic_slice.11 = f32[512]{0:T(512)} dynamic-slice(f32[2048]{0:T(1024)} %param.30, s32[]{:T(128)S(6)} %select_n.38), dynamic_slice_sizes={512} | dynamic-slice | bytes 4100 | tf_op jit(solution)/shard_map/dynamic_slice | solution.py:401
  4.4 0.9 copy.39
  5.3 0.9 copy.40
  6.9 15.6 %shard_map.221 = (bf16[8,256,128]{2,1,0:T(8,128)(2,1)}, s32[8,4,48]{2,1,0:T(4,128)}, f32[8,4,48]{2,1,0:T(4,128)}, bf16[48,256]{1,0:T(8,128)(2,1)}, bf16[48,256]{...) custom-call(bf16[256,128]{1,0:T(8,128)(2,1)} %pad_maximum_fusion.1.refs_0_, s32[4,48]{1,0:T(4,128)} %bitcast.101, ...), custom_call_target="tpu_custom_call" | custom-call | tf_op jit(solution)/shard_map/pallas_call | solution.py:248
  26.3 0.8 reshape.296
  27.1 0.8 reshape.305
  30.2 9.2 %multiply_add_fusion = (f32[48,4,64,64]{3,2,1,0:T(8,128)}, f32[48,4,64]{2,1,0:T(4,128)S(1)}) fusion(f32[48,4,64,64]{3,2,1,0:T(8,128)} %param.23, f32[48,4,64]{2,1,0:T(4,128)S(1)} %reshape.296, f32[48,4,64]{2,1,0:T(4,128)S(1)} %get-tuple-element.27, f32[4]{0:T(128)} %copy-done.14, f32[48,4,64]{2,1,0:T(4,128)S(1)} %get-tuple-element.28), kind=kLoop, calls=%fused_computation | loop fusion | flops 3919872 | bytes 6488080 | tf_op jit(solution)/shard_map/add | solution.py:59
  40.0 1.4 %fusion.53.refs_0_ = bf16[48,256]{1,0:T(8,128)(2,1)} fusion(bf16[48,256]{1,0:T(8,128)(2,1)} %get-tuple-element.15, f32[48,256]{1,0:T(8,128)S(1)} %mul.334, f32[48,256]{1,0:T(8,128)S(1)} %reduce_sum.121, f32[48,256]{1,0:T(8,128)} %mul.320, f32[256]{0:T(256)} %mul.324, bf16[48,256]{1,0:T(8,128)(2,1)} %get-tuple-element.14), kind=kLoop, calls=%fused_computation.76 | loop fusion | flops 147456 | bytes 222208 | tf_op jit(solution)/shard_map/convert_element_type | solution.py:65
  41.4 6.5 %shard_map.222 = bf16[4,48,256]{2,1,0:T(8,128)(2,1)} custom-call(bf16[48,256]{1,0:T(8,128)(2,1)} %fusion.53.refs_0_), custom_call_target="tpu_custom_call" | custom-call | tf_op jit(solution)/shard_map/pallas_call | solution.py:130
  48.7 1.2 fusion.79
  50.5 5.8 %shard_map.223 = f32[4,2,48]{2,1,0:T(2,128)} custom-call(f32[2,48]{1,0:T(2,128)} %pad_maximum_fusion.2.refs_0_), custom_call_target="tpu_custom_call" | custom-call | tf_op jit(solution)/shard_map/pallas_call | solution.py:130
  57.8 17.7 %shard_map.224 = bf16[8,48,2048]{2,1,0:T(8,128)(2,1)} custom-call(bf16[48,512]{1,0:T(8,128)(2,1)} %multiply_convert_fusion.1.source), custom_call_target="tpu_custom_call" | custom-call | tf_op jit(solution)/shard_map/pallas_call | solution.py:321
  75.5 1.5 %fusion.27 = f32[48,128]{1,0:T(8,128)S(1)} fusion(bf16[2048,128]{1,0:T(8,128)(2,1)} %bitcast.91, bf16[8,48,2048]{2,1,0:T(8,128)(2,1)} %shard_map.224, s32[]{:T(128)S(6)} %select_n.43), kind=kOutput, calls=%fused_computation.35 | convolution fusion | flops 25165824 | bytes 745476 | tf_op jit(solution)/shard_map/dot_general | solution.py:442
  77.7 1.1 multiply_reduce_fusion.1
  78.8 1.4 %fusion.30 = f32[48,128]{1,0:T(8,128)S(1)} fusion(bf16[2048,128]{1,0:T(8,128)(2,1)} %param.36, bf16[8,48,2048]{2,1,0:T(8,128)(2,1)} %shard_map.224, s32[]{:T(128)S(6)} %select_n.43), kind=kOutput, calls=%fused_computation.38 | convolution fusion | flops 25165824 | bytes 745476 | tf_op jit(solution)/shard_map/dot_general | solution.py:447
  80.1 1.7 %fusion.4.refs_1_ = bf16[48,128]{1,0:T(8,128)(2,1)} fusion(bf16[2048,128]{1,0:T(8,128)(2,1)S(1)} %copy-done.4, bf16[8,48,2048]{2,1,0:T(8,128)(2,1)} %shard_map.224, s32[]{:T(128)S(6)} %select_n.43, f32[48,128]{1,0:T(8,128)S(1)} %fusion.30), kind=kOutput, calls=%fused_computation.14 | convolution fusion | flops 25202688 | bytes 757764 | tf_op jit(solution)/shard_map/dot_general | solution.py:448
  81.9 1.4 %convolution_convert_fusion = bf16[576,2048]{1,0:T(8,128)(2,1)S(1)} fusion(pred[576,384]{1,0:T(8,128)(4,1)S(1)} %bitcast.93, bf16[384,2048]{1,0:T(8,128)(2,1)S(1)} %bitcast.88), kind=kOutput, calls=%fused_computation.2 | convolution fusion | flops 907149312 | bytes 4153344 | tf_op jit(solution)/shard_map/dot_general | solution.py:434
  85.1 1.5 %fusion.2 = bf16[4,144,128]{2,1,0:T(8,128)(2,1)} fusion(bf16[4,144,2048]{2,1,0:T(8,128)(2,1)S(1)} %bitcast.90, bf16[4,2048,128]{2,1,0:T(8,128)(2,1)S(1)} %copy-done.18, f32[4,144,128]{2,1,0:T(8,128)S(1)} %fusion.81, f32[4,144]{1,0:T(4,128)S(1)} %copy-done.16), kind=kOutput, calls=%fused_computation.8 | convolution fusion | flops 302505984 | bytes 4901120 | tf_op jit(solution)/shard_map/jcd,jdf->jcf/dot_general | solution.py:439
  86.6 12.9 %shard_map.225 = (bf16[4,576,128]{2,1,0:T(8,128)(2,1)}, bf16[4,48,128]{2,1,0:T(8,128)(2,1)}, bf16[4,48,64]{2,1,0:T(8,128)(2,1)}) custom-call(bf16[576,128]{1,0:T(8,128)(2,1)} %bitcast.98, bf16[48,128]{1,0:T(8,128)(2,1)} %fusion.4.refs_1_, bf16[48,64]{1,0:T(8,128)(2,1)} %fusion.55.refs_2_), custom_call_target="tpu_custom_call" | custom-call | tf_op jit(solution)/shard_map/pallas_call | solution.py:130
  99.5 1.2 fusion.80
  100.7 1.6 %fusion = bf16[384,512]{1,0:T(8,128)(2,1)} fusion(bf16[4,512,512]{2,1,0:T(8,128)(2,1)S(1)} %copy-done, bf16[4,144,128]{2,1,0:T(8,128)(2,1)S(1)} %bitcast.95, bf16[4,144,128]{2,1,0:T(8,128)(2,1)S(1)} %bitcast.96, bf16[4,144,128]{2,1,0:T(8,128)(2,1)S(1)} %bitcast.97, bf16[4,144,128]{2,1,0:T(8,128)(2,1)S(1)} %bitcast.94, s32[4,384]{1,0:T(4,128)S(1)} %fusion.6), kind=kOutput, calls=%fused_computation.5 | convolution fusion | flops 531554304 | bytes 3086336 | tf_op jit(solution)/shard_map/dot_general | solution.py:460
  102.3 11.8 %shard_map.226 = bf16[8,48,512]{2,1,0:T(8,128)(2,1)} custom-call(bf16[8,48,512]{2,1,0:T(8,128)(2,1)} %bitcast.92), custom_call_target="tpu_custom_call" | custom-call | tf_op jit(solution)/shard_map/pallas_call | solution.py:167
  114.1 1.1 convert_reduce_fusion
  116.3 5.8 %shard_map.227 = f32[4,2,48]{2,1,0:T(2,128)} custom-call(f32[2,48]{1,0:T(2,128)} %pad_maximum_fusion.3.refs_0_), custom_call_target="tpu_custom_call" | custom-call | tf_op jit(solution)/shard_map/pallas_call | solution.py:130
  (85 shorter events, 17.4 us)
Async XLA Ops:
  0.6 100.0 %copy-start = (bf16[4,512,512]{2,1,0:T(8,128)(2,1)S(1)}, bf16[4,512,512]{2,1,0:T(8,128)(2,1)}, u32[]{:S(2)}) copy-start(bf16[4,512,512]{2,1,0:T(8,128)(2,1)} %param.35) | copy-start | bytes 6291460
  0.7 2.2 %copy-start.14 = (f32[4]{0:T(128)}, f32[4]{0:T(128)S(1)}, u32[]{:S(2)}) copy-start(f32[4]{0:T(128)S(1)} %power_subtract_fusion) | copy-start | bytes 52
  28.5 1.7 %copy-start.9 = (f32[48,4]{1,0:T(8,128)}, f32[48,4]{1,0:T(8,128)S(1)}, u32[]{:S(2)}) copy-start(f32[48,4]{1,0:T(8,128)S(1)} %get-tuple-element.26) | copy-start | bytes 2308
  30.2 9.2 %copy-start.10 = (f32[48,4]{1,0:T(8,128)S(1)}, f32[48,4]{1,0:T(8,128)}, u32[]{:S(2)}) copy-start(f32[48,4]{1,0:T(8,128)} %copy-done.9) | copy-start | bytes 2308
  30.2 9.2 %copy-start.15 = (f32[4]{0:T(128)S(1)}, f32[4]{0:T(128)}, u32[]{:S(2)}) copy-start(f32[4]{0:T(128)} %copy-done.14) | copy-start | bytes 52
  30.2 18.5 %copy-start.3 = (bf16[1024,512]{1,0:T(8,128)(2,1)S(1)}, bf16[1024,512]{1,0:T(8,128)(2,1)}, u32[]{:S(2)}) copy-start(bf16[1024,512]{1,0:T(8,128)(2,1)} %param.29) | copy-start | bytes 3145732
  39.4 17.7 %copy-start.13 = (f32[512]{0:T(512)S(1)}, f32[512]{0:T(512)}, u32[]{:S(2)}) copy-start(f32[512]{0:T(512)} %dynamic_slice.11) | copy-start | bytes 6148
  49.9 30.2 %copy-start.4 = (bf16[2048,128]{1,0:T(8,128)(2,1)S(1)}, bf16[2048,128]{1,0:T(8,128)(2,1)}, u32[]{:S(2)}) copy-start(bf16[2048,128]{1,0:T(8,128)(2,1)} %param.37) | copy-start | bytes 1572868
  57.8 24.1 %copy-start.8 = (pred[4,144,384]{2,1,0:T(8,128)(4,1)S(1)}, pred[4,144,384]{2,1,0:T(8,128)(4,1)}, u32[]{:S(2)}) copy-start(pred[4,144,384]{2,1,0:T(8,128)(4,1)} %iota_compare_fusion) | copy-start | bytes 663556
  75.5 6.4 %copy-start.1 = (bf16[8,48,2048]{2,1,0:T(8,128)(2,1)S(1)}, bf16[8,48,2048]{2,1,0:T(8,128)(2,1)}, u32[]{:S(2)}) copy-start(bf16[8,48,2048]{2,1,0:T(8,128)(2,1)} %shard_map.224) | copy-start | bytes 4718596
  81.9 1.6 %copy-start.2 = (bf16[4,2048,128]{2,1,0:T(8,128)(2,1)S(1)}, bf16[4,2048,128]{2,1,0:T(8,128)(2,1)}, u32[]{:S(2)}) copy-start(bf16[4,2048,128]{2,1,0:T(8,128)(2,1)} %param.33) | copy-start | bytes 6291460
  83.5 0.8 copy-start.16
  83.5 1.6 %copy-start.18 = (bf16[4,2048,128]{2,1,0:T(8,128)(2,1)S(1)}, bf16[4,2048,128]{2,1,0:T(8,128)(2,1)}, u32[]{:S(2)}) copy-start(bf16[4,2048,128]{2,1,0:T(8,128)(2,1)} %param.34) | copy-start | bytes 6291460
  100.7 14.4 %copy-start.12 = (bf16[4,48,128]{2,1,0:T(8,128)(2,1)S(1)}, bf16[4,48,128]{2,1,0:T(8,128)(2,1)}, u32[]{:S(2)}) copy-start(bf16[4,48,128]{2,1,0:T(8,128)(2,1)} %get-tuple-element.20) | copy-start | bytes 147460
  100.7 14.4 %copy-start.5 = (bf16[512,512]{1,0:T(8,128)(2,1)S(1)}, bf16[512,512]{1,0:T(8,128)(2,1)}, u32[]{:S(2)}) copy-start(bf16[512,512]{1,0:T(8,128)(2,1)} %param.38) | copy-start | bytes 1572868
  100.7 14.4 %copy-start.6 = (bf16[48,512]{1,0:T(8,128)(2,1)S(1)}, bf16[48,512]{1,0:T(8,128)(2,1)}, u32[]{:S(2)}) copy-start(bf16[48,512]{1,0:T(8,128)(2,1)} %multiply_convert_fusion.1.source) | copy-start | bytes 147460
  102.3 13.1 %copy-start.11 = (bf16[4,48,64]{2,1,0:T(8,128)(2,1)S(1)}, bf16[4,48,64]{2,1,0:T(8,128)(2,1)}, u32[]{:S(2)}) copy-start(bf16[4,48,64]{2,1,0:T(8,128)(2,1)} %get-tuple-element.21) | copy-start | bytes 73732
  102.3 13.1 %copy-start.7 = (bf16[256,512]{1,0:T(8,128)(2,1)S(1)}, bf16[256,512]{1,0:T(8,128)(2,1)}, u32[]{:S(2)}) copy-start(bf16[256,512]{1,0:T(8,128)(2,1)} %param.41) | copy-start | bytes 786436
  102.3 20.5 %copy-start.17 = (f32[512]{0:T(512)S(1)}, f32[512]{0:T(512)}, u32[]{:S(2)}) copy-start(f32[512]{0:T(512)} %param.43) | copy-start | bytes 6148
